TPU v7x, 32 devices: a whole 2x2x4 slice. The times are simulated.
32 devices in a mesh: fs: 8 (over z, y), tp: 4 (over x, core).
Axes of the slice: x: 2, y: 2, z: 4, core: 2. Of those that a mesh axis runs over, the one named last changes fastest.
Arguments:
- saved_input: bfloat16 [65536, 2048], P(('fs', 'tp')), may hold values from -500 to 500
- value_cotangent: bfloat16 [65536, 1024], P(('fs', 'tp')), may hold values from -500 to 500
- hidden_input: bfloat16 [65536, 1024], P(('fs', 'tp')), may hold values from -500 to 500
- out_cotangent: bfloat16 [65536, 2048], P(('fs', 'tp')), may hold values from -500 to 500
- value_factor: bfloat16 [2048, 256], P('fs'), may hold values from -2 to 2
- out_factor: bfloat16 [1024, 256], P('fs'), may hold values from -2 to 2
- value_weight: float32 [2048, 1024], P('fs', 'tp'), may hold values from -0.125 to 0.125
- out_weight: float32 [1024, 2048], P('fs', 'tp'), may hold values from -0.1875 to 0.1875
- value_first: float32 [256, 1024], P('fs', 'tp'), may hold values from -1.2 to 1.2
- value_second: float32 [256, 1024], P('fs', 'tp'), may hold values from 0.02 to 0.5
- out_first: float32 [256, 2048], P('fs', 'tp'), may hold values from -1.2 to 1.2
- out_second: float32 [256, 2048], P('fs', 'tp'), may hold values from 0.02 to 0.5
Outputs:
- value_update: float32 [2048, 1024], P('fs', 'tp')
- out_update: float32 [1024, 2048], P('fs', 'tp')
- new_value_weight: float32 [2048, 1024], P('fs', 'tp')
- new_out_weight: float32 [1024, 2048], P('fs', 'tp')
- value_copy: bfloat16 [2048, 1024], P(None, 'tp')
- out_copy: bfloat16 [1024, 2048], P(None, 'tp')
- new_value_first: float32 [256, 1024], P('fs', 'tp')
- new_value_second: float32 [256, 1024], P('fs', 'tp')
- new_out_first: float32 [256, 2048], P('fs', 'tp')
- new_out_second: float32 [256, 2048], P('fs', 'tp')
All inputs are finite; a program needn't handle non-finite values.
Results may differ from a plain program's by a relative error of at most 0.0065.
Values may be sent and summed in bfloat16 or wider, within the bound.
A program may use at most 128 MiB of HBM per device.

v0:
```python
import jax
import jax.numpy as jnp
from jax import lax
from jax.sharding import PartitionSpec as P

D = 2048
DM = 1024
R = 256


momentum_decay = 0.9
square_decay = 0.95
adam_epsilon = 1e-08
update_scale = 0.25
learning_rate = 0.01


def moment_ratio(first, second, lowrank, clip_factor):
    scaled = clip_factor * lowrank
    new_first = momentum_decay * first + (1.0 - momentum_decay) * scaled
    new_second = square_decay * second + (1.0 - square_decay) * scaled * scaled
    ratio = new_first / (jnp.sqrt(new_second) + adam_epsilon)
    return (new_first, new_second, ratio)


def input_times_factor(inputs, factor):
    return jnp.dot(
        inputs, lax.all_gather(factor, "fs", axis=0, tiled=True), preferred_element_type=jnp.float32
    )


def split_product(basis, cotangents):
    basis_high = basis.astype(jnp.bfloat16)
    basis_rest = (basis - basis_high.astype(jnp.float32)).astype(jnp.bfloat16)
    high_part = jnp.einsum("tr,tc->rc", basis_high, cotangents, preferred_element_type=jnp.float32)
    rest_part = jnp.einsum("tr,tc->rc", basis_rest, cotangents, preferred_element_type=jnp.float32)
    return high_part + rest_part


def shards(
    saved_input,
    value_cotangent,
    hidden_input,
    out_cotangent,
    value_factor,
    out_factor,
    value_weight,
    out_weight,
    value_first,
    value_second,
    out_first,
    out_second,
):
    highest = lax.Precision.HIGHEST
    value_basis = input_times_factor(saved_input, value_factor)
    out_basis = input_times_factor(hidden_input, out_factor)
    left = value_basis
    right = out_basis
    first_part = split_product(left, value_cotangent)
    second_part = split_product(right, out_cotangent)
    lowrank = lax.psum_scatter(
        jnp.concatenate([first_part, second_part], axis=1), "fs", scatter_dimension=0, tiled=True
    )
    low_value, low_out = (
        lax.psum_scatter(lowrank[:, :DM], "tp", scatter_dimension=1, tiled=True),
        lax.psum_scatter(lowrank[:, DM:], "tp", scatter_dimension=1, tiled=True),
    )
    squares = lax.psum((jnp.sum(low_value * low_value), jnp.sum(low_out * low_out)), ("fs", "tp"))
    root_mean = jnp.sqrt((squares[0] + squares[1]) / (R * (D + DM)))
    clip_factor = 1.0 / jnp.maximum(root_mean, 1.0)
    new_value_first, new_value_second, value_ratio = moment_ratio(
        value_first, value_second, low_value, clip_factor
    )
    new_out_first, new_out_second, out_ratio = moment_ratio(
        out_first, out_second, low_out, clip_factor
    )
    left = value_factor.astype(jnp.float32)
    right = out_factor.astype(jnp.float32)
    value_sum = jnp.dot(
        left, lax.all_gather(value_ratio, "fs", axis=0, tiled=True), precision=highest
    )
    out_sum = jnp.dot(right, lax.all_gather(out_ratio, "fs", axis=0, tiled=True), precision=highest)
    value_update = update_scale * value_sum
    out_update = update_scale * out_sum
    new_value_weight = value_weight - learning_rate * value_update
    new_out_weight = out_weight - learning_rate * out_update
    value_copy, out_copy = (
        lax.all_gather(new_value_weight.astype(jnp.bfloat16), "fs", axis=0, tiled=True),
        lax.all_gather(new_out_weight.astype(jnp.bfloat16), "fs", axis=0, tiled=True),
    )
    return (
        value_update,
        out_update,
        new_value_weight,
        new_out_weight,
        value_copy,
        out_copy,
        new_value_first,
        new_value_second,
        new_out_first,
        new_out_second,
    )


def solution(mesh):
    placed = (
        P(("fs", "tp"), None),
        P(("fs", "tp"), None),
        P(("fs", "tp"), None),
        P(("fs", "tp"), None),
        P("fs", None),
        P("fs", None),
        P("fs", "tp"),
        P("fs", "tp"),
        P("fs", "tp"),
        P("fs", "tp"),
        P("fs", "tp"),
        P("fs", "tp"),
    )
    return jax.shard_map(
        shards,
        mesh=mesh,
        in_specs=placed,
        out_specs=(
            P("fs", "tp"),
            P("fs", "tp"),
            P("fs", "tp"),
            P("fs", "tp"),
            P(None, "tp"),
            P(None, "tp"),
            P("fs", "tp"),
            P("fs", "tp"),
            P("fs", "tp"),
            P("fs", "tp"),
        ),
        check_vma=False,
    )
```

profile of v0, /device:TPU:0, one launch (start us, length us, event | category | flops | bytes accessed | tf_op | source)
XLA Modules:
  0.0 351.5 jit_solution(5440025133149684813)
XLA Ops:
  8.0 33.6 %all_gather.19 = bf16[1024,256]{1,0:T(8,128)(2,1)S(1)} all-gather(bf16[128,256]{1,0:T(8,128)(2,1)} %param.17), channel_id=1, replica_groups=mesh['fs'=8,'tp'=4] {'fs'}, dimensions={0}, use_global_device_ids=true | all-gather | bytes 589824 | tf_op jit(solution)/shard_map/all_gather | solution.py:28
  41.6 3.4 fusion.13
  45.1 2.3 fusion.1
  47.4 2.4 convolution_add_fusion
  49.8 4.3 %all-gather.4.cloned.1.call-done = bf16[2048,256]{1,0:T(8,128)(2,1)} async-done(((bf16[256,256]{1,0:T(8,128)(2,1)}), bf16[2048,256]{1,0:T(8,128)(2,1)}) %all-gather.4.cloned.1.call-update) | async-done | bytes 1048592 | tf_op jit(solution)/shard_map/all_gather | solution.py:28
  54.1 6.2 %fusion.12 = f32[2048,256]{1,0:T(8,128)S(1)} fusion(bf16[2048,2048]{1,0:T(8,128)(2,1)} %param.12, bf16[2048,256]{1,0:T(8,128)(2,1)} %all-gather.4.cloned.1.call-done), kind=kOutput, calls=%fused_computation.27 | convolution fusion | flops 2147483648 | bytes 11534336 | tf_op jit(solution)/shard_map/dot_general | solution.py:27
  60.3 1.3 fusion.4
  62.9 1.9 pad_maximum_fusion
  64.9 73.3 %reduce-scatter.4.cloned.1.call-done = f32[32,3072]{1,0:T(8,128)} async-done(((f32[256,3072]{1,0:T(8,128)}), f32[32,3072]{1,0:T(8,128)}) %reduce-scatter.4.cloned.1.call-update) | async-done | bytes 393232 | tf_op jit(solution)/shard_map/reduce_scatter | solution.py:61
  138.3 1.6 slice.8
  139.9 1.7 slice.9
  141.7 18.4 %reduce-scatter.6.cloned.1.call-done = f32[32,256]{1,0:T(8,128)} async-done(((f32[32,1024]{1,0:T(8,128)}), f32[32,256]{1,0:T(8,128)}) %reduce-scatter.6.cloned.1.call-update) | async-done | bytes 32784 | tf_op jit(solution)/shard_map/reduce_scatter | solution.py:65
  160.1 1.4 multiply_reduce_fusion.1
  161.5 21.6 %reduce-scatter.8.cloned.1.call-done = f32[32,512]{1,0:T(8,128)} async-done(((f32[32,2048]{1,0:T(8,128)}), f32[32,512]{1,0:T(8,128)}) %reduce-scatter.8.cloned.1.call-update) | async-done | bytes 65552 | tf_op jit(solution)/shard_map/reduce_scatter | solution.py:66
  183.1 1.5 multiply_reduce_fusion
  186.0 39.3 %psum.16 = f32[]{:T(128)} all-reduce(f32[]{:T(128)S(6)} %add.45), channel_id=1, replica_groups=mesh['fs'=8,'tp'=4] {'fs','tp'}, use_global_device_ids=true, to_apply=%region_3.0 | all-reduce | flops 1 | bytes 8 | tf_op jit(solution)/shard_map/psum | solution.py:68
  226.0 1.5 add_divide_fusion
  227.6 31.2 %all_gather.21 = f32[256,512]{1,0:T(8,128)S(1)} all-gather(f32[32,512]{1,0:T(8,128)S(1)} %get-tuple-element.24), channel_id=1, replica_groups=mesh['fs'=8,'tp'=4] {'fs'}, dimensions={0}, use_global_device_ids=true | all-gather | bytes 589824 | tf_op jit(solution)/shard_map/all_gather | solution.py:82
  258.8 1.3 fusion.8
  261.0 31.0 %all_gather.20 = f32[256,256]{1,0:T(8,128)S(1)} all-gather(f32[32,256]{1,0:T(8,128)S(1)} %get-tuple-element.27), channel_id=1, replica_groups=mesh['fs'=8,'tp'=4] {'fs'}, dimensions={0}, use_global_device_ids=true | all-gather | bytes 294912 | tf_op jit(solution)/shard_map/all_gather | solution.py:80
  296.4 5.1 %all-gather.8.cloned.1.call-done = bf16[1024,512]{0,1:T(8,128)(2,1)} async-done(((bf16[128,512]{0,1:T(8,128)(2,1)}), bf16[1024,512]{0,1:T(8,128)(2,1)}) %all-gather.8.cloned.1.call-update) | async-done | bytes 1048592 | tf_op jit(solution)/shard_map/all_gather | solution.py:89
  301.5 2.3 copy.29
  303.8 38.6 %all-gather.6.cloned.1.call-done = bf16[2048,256]{0,1:T(8,128)(2,1)} async-done(((bf16[256,256]{0,1:T(8,128)(2,1)}), bf16[2048,256]{0,1:T(8,128)(2,1)}) %all-gather.6.cloned.1.call-update) | async-done | bytes 1048592 | tf_op jit(solution)/shard_map/all_gather | solution.py:88
  342.4 2.3 copy.28
  (45 shorter events, 7.7 us)
Async XLA Ops:
  7.2 46.9 %all-gather.4.cloned.1.call-start = ((), (), s32[]{:S(2)}) async-start(), calls=%async_computation.3 | async-start | bytes 1179648 | tf_op jit(solution)/shard_map/all_gather | solution.py:28
  7.9 130.4 %reduce-scatter.4.cloned.1.call-start = ((), (), s32[]{:S(2)}) async-start(), calls=%async_computation.4 | async-start | bytes 3538944 | tf_op jit(solution)/shard_map/reduce_scatter | solution.py:61
  8.0 37.1 %copy-start = (bf16[2048,2048]{1,0:T(8,128)(2,1)S(1)}, bf16[2048,2048]{1,0:T(8,128)(2,1)}, u32[]{:S(2)}) copy-start(bf16[2048,2048]{1,0:T(8,128)(2,1)} %param.15) | copy-start | bytes 25165828
  54.1 6.3 %copy-start.10 = (bf16[2048,1024]{1,0:T(8,128)(2,1)S(1)}, bf16[2048,1024]{1,0:T(8,128)(2,1)}, u32[]{:S(2)}) copy-start(bf16[2048,1024]{1,0:T(8,128)(2,1)} %param.13) | copy-start | bytes 12582916
  64.8 121.0 %copy-start.3 = (f32[128,512]{1,0:T(8,128)S(1)}, f32[128,512]{1,0:T(8,128)}, u32[]{:S(2)}) copy-start(f32[128,512]{1,0:T(8,128)} %param.19) | copy-start | bytes 786436
  64.8 161.2 %copy-start.6 = (f32[32,512]{1,0:T(8,128)S(1)}, f32[32,512]{1,0:T(8,128)}, u32[]{:S(2)}) copy-start(f32[32,512]{1,0:T(8,128)} %param.23) | copy-start | bytes 196612
  64.8 161.2 %copy-start.7 = (f32[32,512]{1,0:T(8,128)S(1)}, f32[32,512]{1,0:T(8,128)}, u32[]{:S(2)}) copy-start(f32[32,512]{1,0:T(8,128)} %param.22) | copy-start | bytes 196612
  64.8 194.0 %copy-start.2 = (bf16[128,256]{1,0:T(8,128)(2,1)S(1)}, bf16[128,256]{1,0:T(8,128)(2,1)}, u32[]{:S(2)}) copy-start(bf16[128,256]{1,0:T(8,128)(2,1)} %param.17) | copy-start | bytes 196612
  64.8 195.3 %copy-start.4 = (f32[256,256]{1,0:T(8,128)S(1)}, f32[256,256]{1,0:T(8,128)}, u32[]{:S(2)}) copy-start(f32[256,256]{1,0:T(8,128)} %param.18) | copy-start | bytes 786436
  64.8 195.4 %copy-start.8 = (f32[32,256]{1,0:T(8,128)S(1)}, f32[32,256]{1,0:T(8,128)}, u32[]{:S(2)}) copy-start(f32[32,256]{1,0:T(8,128)} %param.21) | copy-start | bytes 98308
  64.9 195.4 %copy-start.9 = (f32[32,256]{1,0:T(8,128)S(1)}, f32[32,256]{1,0:T(8,128)}, u32[]{:S(2)}) copy-start(f32[32,256]{1,0:T(8,128)} %param.20) | copy-start | bytes 98308
  64.9 227.1 %copy-start.1 = (bf16[256,256]{1,0:T(8,128)(2,1)S(1)}, bf16[256,256]{1,0:T(8,128)(2,1)}, u32[]{:S(2)}) copy-start(bf16[256,256]{1,0:T(8,128)(2,1)} %param.16) | copy-start | bytes 393220
  64.9 95.2 %reduce-scatter.6.cloned.1.call-start = ((), (), s32[]{:S(2)}) async-start(), calls=%async_computation.5 | async-start | bytes 163840 | tf_op jit(solution)/shard_map/reduce_scatter | solution.py:65
  139.9 43.2 %reduce-scatter.8.cloned.1.call-start = ((), (), s32[]{:S(2)}) async-start(), calls=%async_computation.6 | async-start | bytes 327680 | tf_op jit(solution)/shard_map/reduce_scatter | solution.py:66
  141.6 159.9 %all-gather.8.cloned.1.call-start = ((), (), s32[]{:S(2)}) async-start(), calls=%async_computation.8 | async-start | bytes 1179648 | tf_op jit(solution)/shard_map/all_gather | solution.py:89
  160.1 100.2 %copy-start.5 = (f32[32,256]{1,0:T(8,128)S(1)}, f32[32,256]{1,0:T(8,128)}, u32[]{:S(2)}) copy-start(f32[32,256]{1,0:T(8,128)} %reduce-scatter.6.cloned.1.call-done) | copy-start | bytes 98308
  260.1 82.4 %all-gather.6.cloned.1.call-start = ((), (), s32[]{:S(2)}) async-start(), calls=%async_computation.7 | async-start | bytes 1179648 | tf_op jit(solution)/shard_map/all_gather | solution.py:88
Sparse Core Ops, SparseCore 0:
  10.1 43.9 all-gather.3
  65.0 73.2 reduce-scatter.3
  141.3 18.7 reduce-scatter.5
  162.9 20.0 reduce-scatter.7
  260.2 41.2 all-gather.7
  304.0 38.3 all-gather.5
where the time goes:
time: 352 us
  waiting for transfers between devices  162 us (46%)
  blocking collectives  135 us (38%)
  matrix products  19.3 us (5%)
  between operations  16.3 us (5%)
  local copies, waits for them, and re-layouts  11.4 us (3%)
  other arithmetic  7.01 us (2%)
    reduce_scatter x1, waiting for transfers between devices, shards(): lax.psum_scatter(jnp.concatenate([first_part, second_part], axis=1), 'fs'...  73.3 us
    psum x1, blocking collectives, shards(): lax.psum((jnp.sum(low_value * low_value), jnp.sum(low_out * low_out)), ('...  39.3 us
    all_gather x1, waiting for transfers between devices, shards(): lax.all_gather(new_value_weight.astype(jnp.bfloat16), 'fs', axis=0, tiled...  38.6 us
    all_gather x1, blocking collectives, input_times_factor(): lax.all_gather(factor, 'fs', axis=0, tiled=True)  33.6 us
    all_gather x1, blocking collectives, shards(): lax.all_gather(out_ratio, 'fs', axis=0, tiled=True)  31.2 us
    all_gather x1, blocking collectives, shards(): lax.all_gather(value_ratio, 'fs', axis=0, tiled=True)  31 us
    reduce_scatter x1, waiting for transfers between devices, shards(): lax.psum_scatter(lowrank[:, DM:], 'tp', scatter_dimension=1, tiled=True)  21.6 us
    reduce_scatter x1, waiting for transfers between devices, shards(): lax.psum_scatter(lowrank[:, :DM], 'tp', scatter_dimension=1, tiled=True)  18.4 us
  transfers between devices with their start and end apart: 6, of which 6 were waited for; matrix products, arithmetic and copies ran while one was open for 5% of the time, Pallas kernels for 0%

commit v1 on v0

v1 whole, which is shorter than its diff:
```python
import functools

import jax
import jax.numpy as jnp
from jax import lax
from jax.experimental import pallas as pl
from jax.experimental.pallas import tpu as pltpu
from jax.sharding import PartitionSpec as P

momentum_decay = 0.9
square_decay = 0.95
adam_epsilon = 1e-08
update_scale = 0.25
learning_rate = 0.01

MESH = pl.DeviceIdType.MESH
CORES = 2
LANES = 128
f32 = jnp.float32
bf16 = jnp.bfloat16


def digits(fs, tp):
    xs = tp // CORES
    ys = xs if fs % xs == 0 else 1
    return fs // ys, ys, xs


def exchange_kernel(
    fs, tp,
    x_v, c_v, x_o, c_o, fac_v, fac_o, w_v, w_o, m1_v, m2_v, m1_o, m2_o,
    F, W_v, W_o, R, n1_v, n2_v, n1_o, n2_o,
    xv, cv, xo, co, hi, rest,
    wown_v, wown_o,
    cs_v, cr_v, cs_o, cr_o, keep_v, keep_o,
    xs_v, xr_v, xs_o, xr_o, acc_v, acc_o,
    ys_v, yr_v, ys_o, yr_o, mid_v, mid_o,
    zs_v, zr_v, zs_o, zr_o, sq_s, sq_r,
    load_sem, fa_s, fa_r, fb_s, fb_r, fc_s, fc_r,
    wl_sem, wz_s, wz_r, wy_s, wy_r,
    rc_s, rc_r, rx_s, rx_r, ry_s, ry_r, rz_s, rz_r, sq_ss, sq_rs, ra_s, ra_r,
):
    Z, Y, X = digits(fs, tp)
    n = fs * tp
    f = lax.axis_index("fs")
    t = lax.axis_index("tp")
    z, y = f // Y, f % Y
    x, c = t // CORES, t % CORES
    me = f * tp + t

    def remote(src, dst, ss, rs, fd, td):
        return pltpu.make_async_remote_copy(
            src_ref=src, dst_ref=dst, send_sem=ss, recv_sem=rs,
            device_id={"fs": fd, "tp": td}, device_id_type=MESH)

    loads = [
        pltpu.make_async_copy(a, b, load_sem.at[i])
        for i, (a, b) in enumerate(((x_o, xo), (c_o, co), (x_v, xv), (c_v, cv)))
    ]
    for cp in loads:
        cp.start()

    barrier = pltpu.get_barrier_semaphore()

    @pl.loop(1, n)
    def _(d):
        peer = lax.rem(me + d, n)
        pl.semaphore_signal(
            barrier, inc=1, device_id={"fs": peer // tp, "tp": lax.rem(peer, tp)},
            device_id_type=MESH)

    rv, ro = fac_v.shape[0], fac_o.shape[0]
    F[pl.ds(f, 1), :rv, :] = fac_v[...][None]
    F[pl.ds(f, 1), rv:, :] = fac_o[...][None]
    wown_v[...] = w_v[...].astype(bf16)
    wown_o[...] = w_o[...].astype(bf16)
    pl.semaphore_wait(barrier, n - 1)

    rx = (rv + ro) // X

    def piece(fi, xi, ci):
        return F.at[fi, pl.ds(pl.multiple_of(xi * rx, 16), rx),
                    pl.ds(pl.multiple_of(ci * LANES, LANES), LANES)]

    def half(fi, ci):
        return F.at[fi, :, pl.ds(pl.multiple_of(ci * LANES, LANES), LANES)]

    def fa(d, fi):
        return remote(piece(fi, x, c), piece(fi, x, c), fa_s.at[d - 1], fa_r.at[d - 1],
                      lax.rem(f + d, fs), t)

    for d in range(1, fs):
        fa(d, f).start()

    parts = ((0, wown_v, W_v), (1, wown_o, W_o))
    own_copies = [pltpu.make_async_copy(own, W.at[z, y], wl_sem.at[p]) for p, own, W in parts]
    for cp in own_copies:
        cp.start()

    def wz(p, W, s, up, zb, src=None):
        k = 0 if up else 1
        zd = z + 1 if up else z - 1
        return remote(W.at[zb, y] if src is None else src, W.at[zb, y],
                      wz_s.at[p, k, s], wz_r.at[p, k, s], zd * Y + y, t)

    def wy(p, W, zb, d, yb, src=None):
        return remote(W.at[zb, yb] if src is None else src, W.at[zb, yb],
                      wy_s.at[p, zb, d - 1], wy_r.at[p, zb, d - 1],
                      z * Y + lax.rem(y + d, Y), t)

    def weights_send(s):
        @pl.when((z >= s) & (z < Z - 1))
        def _():
            for p, own, W in parts:
                wz(p, W, s, True, z - s, own if s == 0 else None).start()

        @pl.when((z + s < Z) & (z > 0))
        def _():
            for p, own, W in parts:
                wz(p, W, s, False, z + s, own if s == 0 else None).start()

    def weights_receive(s):
        for up in (True, False):
            zb = z - 1 - s if up else z + 1 + s

            @pl.when((zb >= 0) if up else (zb < Z))
            def _():
                for p, own, W in parts:
                    wz(p, W, s, up, zb).wait_recv()
                    for d in range(1, Y):
                        wy(p, W, zb, d, y).start()

    weights_send(0)
    for p, own, W in parts:
        for d in range(1, Y):
            wy(p, W, z, d, y, own).start()

    def fb(d, k, fi, xi):
        return remote(piece(fi, xi, c), piece(fi, xi, c), fb_s.at[d - 1, k - 1],
                      fb_r.at[d - 1, k - 1], f, lax.rem(x + k, X) * CORES + c)

    def fc(d, fi, ci):
        return remote(half(fi, ci), half(fi, ci), fc_s.at[d - 1], fc_r.at[d - 1],
                      f, x * CORES + 1 - c)

    source = [lax.rem(f + fs - d, fs) for d in range(fs)]
    for d in range(1, fs):
        fa(d, source[d]).wait_recv()
        for k in range(1, X):
            fb(d, k, source[d], x).start()
    for d in range(1, fs):
        for k in range(1, X):
            fb(d, k, source[d], lax.rem(x + X - k, X)).wait_recv()
        fc(d, source[d], c).start()
    for d in range(1, fs):
        fc(d, source[d], 1 - c).wait_recv()

    tokens = xo.shape[0]
    step = tokens // 4

    def basis(x_ref, rows):
        @pl.loop(0, tokens // step)
        def _(i):
            at = pl.ds(pl.multiple_of(i * step, step), step)
            fac = F[:, rows, :].reshape(-1, F.shape[2])
            b = jnp.dot(x_ref[at, :], fac, preferred_element_type=f32).T
            high = b.astype(bf16)
            hi[:, at] = high
            rest[:, at] = (b - high.astype(f32)).astype(bf16)

    def product(c_ref, start, width):
        cols = c_ref[:, pl.ds(pl.multiple_of(start, LANES), width)]
        return (jnp.dot(hi[...], cols, preferred_element_type=f32)
                + jnp.dot(rest[...], cols, preferred_element_type=f32))

    def rc(p, send, recv, i):
        return remote(send.at[i], recv.at[i], rc_s.at[p, i], rc_r.at[p, i],
                      f, x * CORES + 1 - c)

    def multiply(p, c_ref, send, recv, keep):
        cb = keep.shape[2]

        @pl.loop(0, X)
        def _(i):
            send[i] = product(c_ref, (i * CORES + 1 - c) * cb, cb)
            rc(p, send, recv, i).start()

        @pl.loop(0, X)
        def _(i):
            keep[i] = product(c_ref, (i * CORES + c) * cb, cb)

    def sx(p, send, recv, k):
        xd = lax.rem(x + k, X)
        return remote(send.at[k - 1], recv.at[k - 1], rx_s.at[p, k - 1], rx_r.at[p, k - 1],
                      f, xd * CORES + c)

    def sy(p, send, recv, k):
        yd = lax.rem(y + k, Y)
        return remote(send.at[k - 1], recv.at[k - 1], ry_s.at[p, k - 1], ry_r.at[p, k - 1],
                      z * Y + yd, t)

    def sz(p, send, recv, k):
        zd = lax.rem(z + k, Z)
        return remote(send.at[k - 1], recv.at[k - 1], rz_s.at[p, k - 1], rz_r.at[p, k - 1],
                      zd * Y + y, t)

    def to_x(p, cs, cr, keep, send, recv):
        for i in range(X):
            rc(p, cs, cr, i).wait_recv()
        for k in range(1, X):
            xd = lax.rem(x + k, X)
            send[k - 1] = (keep[xd] + cr[xd]).astype(bf16)
            sx(p, send, recv, k).start()

    def to_y(p, cr, keep, xsend, recv, acc, send, yrecv):
        total = keep[x] + cr[x]
        for k in range(1, X):
            sx(p, xsend, recv, k).wait_recv()
            total = total + recv[k - 1].astype(f32)
        acc[...] = total.reshape(acc.shape)
        for k in range(1, Y):
            yd = lax.rem(y + k, Y)
            send[k - 1] = acc[:, pl.ds(yd, 1)][:, 0].astype(bf16)
            sy(p, send, yrecv, k).start()

    def to_z(p, acc, ysend, recv, mid, send, zrecv):
        total = acc[:, pl.ds(y, 1)][:, 0]
        for k in range(1, Y):
            sy(p, ysend, recv, k).wait_recv()
            total = total + recv[k - 1].astype(f32)
        mid[...] = total
        for k in range(1, Z):
            send[k - 1] = mid[lax.rem(z + k, Z)].astype(bf16)
            sz(p, send, zrecv, k).start()

    def finish(p, mid, send, recv):
        total = mid[z]
        for k in range(1, Z):
            sz(p, send, recv, k).wait_recv()
            total = total + recv[k - 1].astype(f32)
        return total

    loads[0].wait()
    basis(xo, slice(rv, rv + ro))
    loads[1].wait()
    multiply(1, co, cs_o, cr_o, keep_o)
    to_x(1, cs_o, cr_o, keep_o, xs_o, xr_o)
    if Z > 1:
        weights_receive(0)
    if Z > 2:
        weights_send(1)
    loads[2].wait()
    basis(xv, slice(0, rv))
    loads[3].wait()
    multiply(0, cv, cs_v, cr_v, keep_v)
    to_x(0, cs_v, cr_v, keep_v, xs_v, xr_v)
    to_y(1, cr_o, keep_o, xs_o, xr_o, acc_o, ys_o, yr_o)
    to_y(0, cr_v, keep_v, xs_v, xr_v, acc_v, ys_v, yr_v)
    to_z(1, acc_o, ys_o, yr_o, mid_o, zs_o, zr_o)
    to_z(0, acc_v, ys_v, yr_v, mid_v, zs_v, zr_v)
    for s in range(1, Z - 1):
        weights_receive(s)
        if s + 1 < Z - 1:
            weights_send(s + 1)
    low_o = finish(1, mid_o, zs_o, zr_o)
    low_v = finish(0, mid_v, zs_v, zr_v)

    square = jnp.sum(low_o * low_o) + jnp.sum(low_v * low_v)
    sq_s[...] = jnp.full(sq_s.shape, square, f32)

    @pl.loop(1, n)
    def _(d):
        peer = lax.rem(me + d, n)
        remote(sq_s, sq_r.at[d - 1], sq_ss.at[d - 1], sq_rs.at[d - 1],
               peer // tp, lax.rem(peer, tp)).start()

    @pl.loop(1, n)
    def _(d):
        remote(sq_s, sq_r.at[d - 1], sq_ss.at[d - 1], sq_rs.at[d - 1], f, t).wait_recv()

    total = jnp.sum(sq_r[...], axis=0)[0:1, 0:1] + square
    count = hi.shape[0] * (cv.shape[1] + co.shape[1])
    clip = 1.0 / jnp.maximum(jnp.sqrt(total / count), 1.0)

    def moments(low, m1, m2, n1, n2):
        scaled = clip * low
        first = momentum_decay * m1[...] + (1.0 - momentum_decay) * scaled
        second = square_decay * m2[...] + (1.0 - square_decay) * scaled * scaled
        n1[...] = first
        n2[...] = second
        return (first / (jnp.sqrt(second) + adam_epsilon)).astype(bf16)

    cbv = low_v.shape[1]
    R[pl.ds(f, 1), :, :cbv] = moments(low_v, m1_v, m2_v, n1_v, n2_v)[None]
    R[pl.ds(f, 1), :, cbv:] = moments(low_o, m1_o, m2_o, n1_o, n2_o)[None]

    def ra(d, fi):
        return remote(R.at[fi], R.at[fi], ra_s.at[d - 1], ra_r.at[d - 1], lax.rem(f + d, fs), t)

    for d in range(1, fs):
        ra(d, f).start()

    for cp in own_copies:
        cp.wait()
    for s in range(Z - 1):
        @pl.when((z >= s) & (z < Z - 1))
        def _():
            for p, own, W in parts:
                wz(p, W, s, True, z - s, own if s == 0 else None).wait_send()

        @pl.when((z + s < Z) & (z > 0))
        def _():
            for p, own, W in parts:
                wz(p, W, s, False, z + s, own if s == 0 else None).wait_send()
    for p, own, W in parts:
        for zb in range(Z):
            for d in range(1, Y):
                wy(p, W, zb, d, y).wait_send()
                wy(p, W, zb, d, lax.rem(y + Y - d, Y)).wait_recv()
    for d in range(1, fs):
        fa(d, f).wait_send()
        for k in range(1, X):
            fb(d, k, source[d], x).wait_send()
        fc(d, source[d], c).wait_send()
    for p, cs, cr, xsnd, xrcv, ysnd, yrcv, zsnd, zrcv in (
        (0, cs_v, cr_v, xs_v, xr_v, ys_v, yr_v, zs_v, zr_v),
        (1, cs_o, cr_o, xs_o, xr_o, ys_o, yr_o, zs_o, zr_o),
    ):
        for i in range(X):
            rc(p, cs, cr, i).wait_send()
        for k in range(1, X):
            sx(p, xsnd, xrcv, k).wait_send()
        for k in range(1, Y):
            sy(p, ysnd, yrcv, k).wait_send()
        for k in range(1, Z):
            sz(p, zsnd, zrcv, k).wait_send()

    @pl.loop(1, n)
    def _(d):
        remote(sq_s, sq_r.at[d - 1], sq_ss.at[d - 1], sq_rs.at[d - 1], f, t).wait_send()

    for d in range(1, fs):
        ra(d, f).wait_send()
        ra(d, source[d]).wait_recv()


def update_kernel(fs, F, R, W_v, W_o, w_v, w_o, u_v, u_o, nw_v, nw_o, copy_v, copy_o):
    f = lax.axis_index("fs")
    rv, ro = w_v.shape[0], w_o.shape[0]
    cbv = w_v.shape[1]
    rank = F.shape[2]
    ratio = R[...].reshape(rank, -1)
    rate = learning_rate * update_scale

    for rows, cols, W, w, u, nw, copy in (
        (slice(0, rv), slice(0, cbv), W_v, w_v, u_v, nw_v, copy_v),
        (slice(rv, rv + ro), slice(cbv, None), W_o, w_o, u_o, nw_o, copy_o),
    ):
        k = w.shape[0]
        fac = F[:, rows, :].reshape(fs * k, rank)
        all_rows = jnp.dot(fac, ratio[:, cols], preferred_element_type=f32)
        copy[...] = (W[...].astype(f32).reshape(all_rows.shape) - rate * all_rows).astype(bf16)
        mine = jnp.dot(F[pl.ds(f, 1), rows, :][0], ratio[:, cols], preferred_element_type=f32)
        update = update_scale * mine
        u[...] = update
        nw[...] = w[...] - learning_rate * update


def solution(mesh):
    fs, tp = mesh.shape["fs"], mesh.shape["tp"]
    Z, Y, X = digits(fs, tp)

    def shards(x_v, c_v, x_o, c_o, fac_v, fac_o, w_v, w_o, m1_v, m2_v, m1_o, m2_o):
        rank = fac_v.shape[1]
        rr = rank // fs
        cbv, cbo = w_v.shape[1], w_o.shape[1]
        tokens = x_v.shape[0]
        vmem = pl.BlockSpec(memory_space=pltpu.VMEM)
        hbm = pl.BlockSpec(memory_space=pl.ANY)
        sds = jax.ShapeDtypeStruct
        V = pltpu.VMEM
        dma = pltpu.SemaphoreType.DMA

        def both(shape_of, dtype, copies=2):
            out = []
            for cb in (cbv, cbo):
                out += [V(shape_of(cb), dtype)] * copies
            return out

        x1, y1, z1 = max(X - 1, 1), max(Y - 1, 1), max(Z - 1, 1)
        scratch = [
            V(x_v.shape, bf16), V(c_v.shape, bf16), V(x_o.shape, bf16), V(c_o.shape, bf16),
            V((rank, tokens), bf16), V((rank, tokens), bf16),
            V(w_v.shape, bf16), V(w_o.shape, bf16),
            *both(lambda cb: (X, rank, cb), f32), *both(lambda cb: (X, rank, cb), f32, 1),
            *both(lambda cb: (x1, rank, cb), bf16),
            *both(lambda cb: (Z, Y, rr, cb), f32, 1),
            *both(lambda cb: (y1, Z, rr, cb), bf16),
            *both(lambda cb: (Z, rr, cb), f32, 1),
            *both(lambda cb: (z1, rr, cb), bf16),
            V((1, LANES), f32), V((fs * tp - 1, 1, LANES), f32),
            dma((4,)), dma((fs - 1,)), dma((fs - 1,)), dma((fs - 1, x1)), dma((fs - 1, x1)),
            dma((fs - 1,)), dma((fs - 1,)),
            dma((2,)), dma((2, 2, z1)), dma((2, 2, z1)), dma((2, Z, y1)), dma((2, Z, y1)),
            dma((2, X)), dma((2, X)), dma((2, x1)), dma((2, x1)), dma((2, y1)), dma((2, y1)),
            dma((2, z1)), dma((2, z1)), dma((fs * tp - 1,)), dma((fs * tp - 1,)),
            dma((fs - 1,)), dma((fs - 1,)),
        ]
        rows = fac_v.shape[0] + fac_o.shape[0]
        F, W_v, W_o, R, n1_v, n2_v, n1_o, n2_o = pl.pallas_call(
            functools.partial(exchange_kernel, fs, tp),
            out_shape=(
                sds((fs, rows, rank), bf16), sds((Z, Y) + w_v.shape, bf16),
                sds((Z, Y) + w_o.shape, bf16), sds((fs, rr, cbv + cbo), bf16),
                sds(m1_v.shape, f32), sds(m2_v.shape, f32),
                sds(m1_o.shape, f32), sds(m2_o.shape, f32),
            ),
            in_specs=[hbm] * 4 + [vmem] * 8,
            out_specs=(vmem, hbm, hbm, vmem, vmem, vmem, vmem, vmem),
            scratch_shapes=scratch,
            compiler_params=pltpu.CompilerParams(
                collective_id=0, has_side_effects=True, vmem_limit_bytes=60 * 1024 * 1024),
            name="exchange",
        )(x_v, c_v, x_o, c_o, fac_v, fac_o, w_v, w_o, m1_v, m2_v, m1_o, m2_o)
        outs = pl.pallas_call(
            functools.partial(update_kernel, fs),
            out_shape=(
                sds(w_v.shape, f32), sds(w_o.shape, f32),
                sds(w_v.shape, f32), sds(w_o.shape, f32),
                sds((fs * w_v.shape[0], cbv), bf16), sds((fs * w_o.shape[0], cbo), bf16),
            ),
            in_specs=[vmem] * 6,
            out_specs=(vmem,) * 6,
            compiler_params=pltpu.CompilerParams(vmem_limit_bytes=48 * 1024 * 1024),
            name="update",
        )(F, R, W_v, W_o, w_v, w_o)
        return (*outs, n1_v, n2_v, n1_o, n2_o)

    fsp = P(("fs", "tp"), None)
    both = P("fs", "tp")
    return jax.shard_map(
        shards,
        mesh=mesh,
        in_specs=(fsp,) * 4 + (P("fs", None),) * 2 + (both,) * 6,
        out_specs=(both,) * 4 + (P(None, "tp"),) * 2 + (both,) * 4,
        check_vma=False,
    )
```

time: 352 us -> 83.1 us (0.24)
  waiting for transfers between devices: 162 us -> 0 us
  blocking collectives: 135 us -> 0 us
  Pallas kernels: 0 us -> 74.8 us
  matrix products: 19.3 us -> 0 us
  between operations: 16.3 us -> 0.71 us
  other arithmetic: 7.01 us -> 0 us
  local copies, waits for them, and re-layouts: 11.4 us -> 7.36 us
    reduce_scatter x3 -> x0, waiting for transfers between devices: 113 us -> none  [the longest x1 73.3 us: shards(): lax.psum_scatter(jnp.concatenate([first_part, second_part], axis=1), 'fs'...]
    all_gather x3 -> x0, blocking collectives: 95.8 us -> none  [the longest x1 33.6 us: input_times_factor(): lax.all_gather(factor, 'fs', axis=0, tiled=True)]
    pallas_call x0 -> x2, Pallas kernels: none -> 74.8 us  [the longest x1 72.4 us: shards(): pl.pallas_call(functools.partial(exchange_kernel, fs, tp), out_shape=(sds...]
    all_gather x3 -> x0, waiting for transfers between devices: 48.1 us -> none  [the longest x1 38.6 us: shards(): lax.all_gather(new_value_weight.astype(jnp.bfloat16), 'fs', axis=0, tiled...]
    psum x1 -> x0, blocking collectives: 39.3 us -> none  [shards(): lax.psum((jnp.sum(low_value * low_value), jnp.sum(low_out * low_out)), ('...]
    dot_general x8 -> x0, matrix products: 19.3 us -> none  [the longest x2 9.69 us: input_times_factor(): jnp.dot(inputs, lax.all_gather(factor, 'fs', axis=0, tiled=True), preferr...]
    unnamed x30 -> x24, local copies, waits for them, and re-layouts: 8.18 us -> 7.36 us
  transfers between devices with their start and end apart: 6 -> 0, of which waited for: 6 -> 0; matrix products, arithmetic and copies ran while one was open for 5% -> 0% of each run, Pallas kernels for 0% -> 0%
where the time goes in v1:
time: 83.1 us; the launch traced here: 82.9 us
  Pallas kernels  74.8 us (90%)
  local copies, waits for them, and re-layouts  7.36 us (9%)
    pallas_call x1, Pallas kernels, shards(): pl.pallas_call(functools.partial(exchange_kernel, fs, tp), out_shape=(sds...  72.4 us
    unnamed x24, local copies, waits for them, and re-layouts  7.36 us
    pallas_call x1, Pallas kernels, shards(): pl.pallas_call(functools.partial(update_kernel, fs), out_shape=(sds(w_v.s...  2.35 us

profile of v1, /device:TPU:0, one launch (start us, length us, event | category | flops | bytes accessed | tf_op | source)
XLA Modules:
  0.0 82.9 jit_solution(12368686436112081519)
XLA Ops:
  0.6 0.0 copy-start.2
  0.7 0.0 copy-start.1
  0.7 72.4 %exchange.1 = (bf16[8,384,256]{2,1,0:T(8,128)(2,1)}, bf16[4,2,256,256]{3,2,1,0:T(8,128)(2,1)}, bf16[4,2,128,512]{3,2,1,0:T(8,128)(2,1)}, bf16[8,32,768]{2,1,0:T(...) custom-call(bf16[2048,2048]{1,0:T(8,128)(2,1)} %x_v.1, ...), custom_call_target="tpu_custom_call" | custom-call | tf_op jit(solution)/shard_map/exchange/pallas_call | solution.py:410
  73.1 0.0 copy-done.2
  73.1 0.0 copy-done.1
  73.1 0.0 copy-start
  73.1 1.4 %copy-done = bf16[8,384,256]{2,1,0:T(8,128)(2,1)S(1)} copy-done((bf16[8,384,256]{2,1,0:T(8,128)(2,1)S(1)}, bf16[8,384,256]{2,1,0:T(8,128)(2,1)}, u32[]{:S(2)}) %copy-start) | copy-done | bytes 1572888
  74.5 0.0 copy-start.3
  74.5 1.2 %copy-done.3 = bf16[4,2,256,256]{3,2,1,0:T(8,128)(2,1)S(1)} copy-done((bf16[4,2,256,256]{3,2,1,0:T(8,128)(2,1)S(1)}, bf16[4,2,256,256]{3,2,1,0:T(8,128)(2,1)}, u32[]{:S(2)}) %copy-start.3) | copy-done | bytes 1048600
  75.8 0.0 copy-start.4
  75.8 1.2 %copy-done.4 = bf16[4,2,128,512]{3,2,1,0:T(8,128)(2,1)S(1)} copy-done((bf16[4,2,128,512]{3,2,1,0:T(8,128)(2,1)S(1)}, bf16[4,2,128,512]{3,2,1,0:T(8,128)(2,1)}, u32[]{:S(2)}) %copy-start.4) | copy-done | bytes 1048600
  77.0 0.0 copy-start.5
  77.0 1.0 %copy-done.5 = bf16[8,32,768]{2,1,0:T(8,128)(2,1)S(1)} copy-done((bf16[8,32,768]{2,1,0:T(8,128)(2,1)S(1)}, bf16[8,32,768]{2,1,0:T(8,128)(2,1)}, u32[]{:S(2)}) %copy-start.5) | copy-done | bytes 393240
  78.0 0.0 copy-start.9
  78.0 0.0 copy-start.8
  78.0 2.4 %update.1 = (f32[256,256]{1,0:T(8,128)}, f32[128,512]{1,0:T(8,128)}, f32[256,256]{1,0:T(8,128)}, f32[128,512]{1,0:T(8,128)}, bf16[2048,256]{1,0:T(8,128)(2,1)}, /*index=5*/bf16[1024,512]{1,0:T(8,128)(2,1)}) custom-call(bf16[8,384,256]{2,1,0:T(8,128)(2,1)S(1)} %copy-done, bf16[8,32,768]{2,1,0:T(8,128)(2,1)S(1)} %copy-done.5, ...), custom_call_target="tpu_custom_call" | custom-call | tf_op jit(solution)/shard_map/update/pallas_call | solution.py:425
  80.4 0.0 copy-done.9
  80.4 0.6 copy.26
  81.0 0.0 copy-done.8
  81.0 0.6 copy.27
  81.6 0.0 copy-done.7
  81.6 0.6 copy.28
  82.2 0.0 copy-done.6
  82.2 0.6 copy.29
  (2 shorter events, 0.0 us)
Async XLA Ops:
  0.6 72.5 %copy-start.2 = (f32[128,512]{1,0:T(8,128)S(1)}, f32[128,512]{1,0:T(8,128)}, u32[]{:S(2)}) copy-start(f32[128,512]{1,0:T(8,128)} %w_o.3) | copy-start | bytes 786436
  0.7 72.5 %copy-start.1 = (f32[256,256]{1,0:T(8,128)S(1)}, f32[256,256]{1,0:T(8,128)}, u32[]{:S(2)}) copy-start(f32[256,256]{1,0:T(8,128)} %w_v.3) | copy-start | bytes 786436
  73.1 1.4 %copy-start = (bf16[8,384,256]{2,1,0:T(8,128)(2,1)S(1)}, bf16[8,384,256]{2,1,0:T(8,128)(2,1)}, u32[]{:S(2)}) copy-start(bf16[8,384,256]{2,1,0:T(8,128)(2,1)} %get-tuple-element.24.F) | copy-start | bytes 4718596
  74.5 1.2 %copy-start.3 = (bf16[4,2,256,256]{3,2,1,0:T(8,128)(2,1)S(1)}, bf16[4,2,256,256]{3,2,1,0:T(8,128)(2,1)}, u32[]{:S(2)}) copy-start(bf16[4,2,256,256]{3,2,1,0:T(8,128)(2,1)} %get-tuple-element.26.W_v) | copy-start | bytes 3145732
  75.8 1.2 %copy-start.4 = (bf16[4,2,128,512]{3,2,1,0:T(8,128)(2,1)S(1)}, bf16[4,2,128,512]{3,2,1,0:T(8,128)(2,1)}, u32[]{:S(2)}) copy-start(bf16[4,2,128,512]{3,2,1,0:T(8,128)(2,1)} %get-tuple-element.27.W_o) | copy-start | bytes 3145732
  77.0 1.0 %copy-start.5 = (bf16[8,32,768]{2,1,0:T(8,128)(2,1)S(1)}, bf16[8,32,768]{2,1,0:T(8,128)(2,1)}, u32[]{:S(2)}) copy-start(bf16[8,32,768]{2,1,0:T(8,128)(2,1)} %get-tuple-element.25.R) | copy-start | bytes 1179652
  78.0 2.4 %copy-start.9 = (f32[32,256]{1,0:T(8,128)S(1)}, f32[32,256]{1,0:T(8,128)}, u32[]{:S(2)}) copy-start(f32[32,256]{1,0:T(8,128)} %get-tuple-element.54) | copy-start | bytes 98308
  78.0 3.0 %copy-start.8 = (f32[32,256]{1,0:T(8,128)S(1)}, f32[32,256]{1,0:T(8,128)}, u32[]{:S(2)}) copy-start(f32[32,256]{1,0:T(8,128)} %get-tuple-element.55) | copy-start | bytes 98308
  78.0 3.6 %copy-start.7 = (f32[32,512]{1,0:T(8,128)S(1)}, f32[32,512]{1,0:T(8,128)}, u32[]{:S(2)}) copy-start(f32[32,512]{1,0:T(8,128)} %get-tuple-element.56) | copy-start | bytes 196612
  78.0 4.2 %copy-start.6 = (f32[32,512]{1,0:T(8,128)S(1)}, f32[32,512]{1,0:T(8,128)}, u32[]{:S(2)}) copy-start(f32[32,512]{1,0:T(8,128)} %get-tuple-element.57) | copy-start | bytes 196612

commit v2 on v1

--- a/solution.py
+++ b/solution.py
@@ -26,10 +26,15 @@
     return fs // ys, ys, xs
 
 
+def moments(scaled, first, second):
+    return (momentum_decay * first + (1.0 - momentum_decay) * scaled,
+            square_decay * second + (1.0 - square_decay) * scaled * scaled)
+
+
 def exchange_kernel(
     fs, tp,
     x_v, c_v, x_o, c_o, fac_v, fac_o, w_v, w_o, m1_v, m2_v, m1_o, m2_o,
-    F, W_v, W_o, R, n1_v, n2_v, n1_o, n2_o,
+    F, W_v, W_o, R, S,
     xv, cv, xo, co, hi, rest,
     wown_v, wown_o,
     cs_v, cr_v, cs_o, cr_o, keep_v, keep_o,
@@ -282,17 +287,14 @@
     count = hi.shape[0] * (cv.shape[1] + co.shape[1])
     clip = 1.0 / jnp.maximum(jnp.sqrt(total / count), 1.0)
 
-    def moments(low, m1, m2, n1, n2):
+    cbv = low_v.shape[1]
+    for cols, low, m1, m2 in (
+        (slice(0, cbv), low_v, m1_v, m2_v), (slice(cbv, None), low_o, m1_o, m2_o)
+    ):
         scaled = clip * low
-        first = momentum_decay * m1[...] + (1.0 - momentum_decay) * scaled
-        second = square_decay * m2[...] + (1.0 - square_decay) * scaled * scaled
-        n1[...] = first
-        n2[...] = second
-        return (first / (jnp.sqrt(second) + adam_epsilon)).astype(bf16)
-
-    cbv = low_v.shape[1]
-    R[pl.ds(f, 1), :, :cbv] = moments(low_v, m1_v, m2_v, n1_v, n2_v)[None]
-    R[pl.ds(f, 1), :, cbv:] = moments(low_o, m1_o, m2_o, n1_o, n2_o)[None]
+        S[:, cols] = scaled
+        first, second = moments(scaled, m1[...], m2[...])
+        R[pl.ds(f, 1), :, cols] = (first / (jnp.sqrt(second) + adam_epsilon)).astype(bf16)[None]
 
     def ra(d, fi):
         return remote(R.at[fi], R.at[fi], ra_s.at[d - 1], ra_r.at[d - 1], lax.rem(f + d, fs), t)
@@ -344,26 +346,41 @@
         ra(d, source[d]).wait_recv()
 
 
-def update_kernel(fs, F, R, W_v, W_o, w_v, w_o, u_v, u_o, nw_v, nw_o, copy_v, copy_o):
+def update_kernel(
+    F, W_v, W_o, R, S, w_v, w_o, m1_v, m2_v, m1_o, m2_o,
+    u_v, u_o, nw_v, nw_o, copy_v, copy_o, n1_v, n2_v, n1_o, n2_o,
+):
     f = lax.axis_index("fs")
+    step = pl.program_id(0)
+    group = F.shape[0]
     rv, ro = w_v.shape[0], w_o.shape[0]
     cbv = w_v.shape[1]
     rank = F.shape[2]
-    ratio = R[...].reshape(rank, -1)
     rate = learning_rate * update_scale
 
-    for rows, cols, W, w, u, nw, copy in (
+    parts = (
         (slice(0, rv), slice(0, cbv), W_v, w_v, u_v, nw_v, copy_v),
         (slice(rv, rv + ro), slice(cbv, None), W_o, w_o, u_o, nw_o, copy_o),
-    ):
-        k = w.shape[0]
-        fac = F[:, rows, :].reshape(fs * k, rank)
-        all_rows = jnp.dot(fac, ratio[:, cols], preferred_element_type=f32)
-        copy[...] = (W[...].astype(f32).reshape(all_rows.shape) - rate * all_rows).astype(bf16)
-        mine = jnp.dot(F[pl.ds(f, 1), rows, :][0], ratio[:, cols], preferred_element_type=f32)
-        update = update_scale * mine
-        u[...] = update
-        nw[...] = w[...] - learning_rate * update
+    )
+    for rows, cols, W, w, u, nw, copy in parts:
+        fac = F[:, rows, :].reshape(-1, rank)
+        ratio = R[...].reshape(rank, -1)[:, cols]
+        change = jnp.dot(fac, ratio, preferred_element_type=f32)
+        copy[...] = (W[...].astype(f32).reshape(change.shape) - rate * change).astype(bf16)
+
+    @pl.when(step == f // group)
+    def _():
+        for rows, cols, W, w, u, nw, copy in parts:
+            ratio = R[...].reshape(rank, -1)[:, cols]
+            mine = jnp.dot(F[pl.ds(f % group, 1), rows, :][0], ratio, preferred_element_type=f32)
+            update = update_scale * mine
+            u[...] = update
+            nw[...] = w[...] - learning_rate * update
+
+    @pl.when(step == 0)
+    def _():
+        n1_v[...], n2_v[...] = moments(S[:, :cbv], m1_v[...], m2_v[...])
+        n1_o[...], n2_o[...] = moments(S[:, cbv:], m1_o[...], m2_o[...])
 
 
 def solution(mesh):
@@ -407,34 +424,52 @@
             dma((fs - 1,)), dma((fs - 1,)),
         ]
         rows = fac_v.shape[0] + fac_o.shape[0]
-        F, W_v, W_o, R, n1_v, n2_v, n1_o, n2_o = pl.pallas_call(
+        F, W_v, W_o, R, S = pl.pallas_call(
             functools.partial(exchange_kernel, fs, tp),
             out_shape=(
                 sds((fs, rows, rank), bf16), sds((Z, Y) + w_v.shape, bf16),
                 sds((Z, Y) + w_o.shape, bf16), sds((fs, rr, cbv + cbo), bf16),
-                sds(m1_v.shape, f32), sds(m2_v.shape, f32),
-                sds(m1_o.shape, f32), sds(m2_o.shape, f32),
+                sds((rr, cbv + cbo), f32),
             ),
             in_specs=[hbm] * 4 + [vmem] * 8,
-            out_specs=(vmem, hbm, hbm, vmem, vmem, vmem, vmem, vmem),
+            out_specs=(vmem, hbm, hbm, vmem, vmem),
             scratch_shapes=scratch,
             compiler_params=pltpu.CompilerParams(
                 collective_id=0, has_side_effects=True, vmem_limit_bytes=60 * 1024 * 1024),
             name="exchange",
         )(x_v, c_v, x_o, c_o, fac_v, fac_o, w_v, w_o, m1_v, m2_v, m1_o, m2_o)
-        outs = pl.pallas_call(
-            functools.partial(update_kernel, fs),
+        group = Y
+
+        def whole(a):
+            return pl.BlockSpec(a.shape, lambda i: (0,) * len(a.shape))
+
+        def tall(a):
+            return pl.BlockSpec((group * a.shape[0], a.shape[1]), lambda i: (i, 0))
+
+        def stack(a):
+            return pl.BlockSpec((1, group) + a.shape, lambda i: (i, 0, 0, 0))
+
+        small = (m1_v, m2_v, m1_o, m2_o)
+        return pl.pallas_call(
+            update_kernel,
+            grid=(fs // group,),
             out_shape=(
                 sds(w_v.shape, f32), sds(w_o.shape, f32),
                 sds(w_v.shape, f32), sds(w_o.shape, f32),
                 sds((fs * w_v.shape[0], cbv), bf16), sds((fs * w_o.shape[0], cbo), bf16),
+                *[sds(a.shape, f32) for a in small],
             ),
-            in_specs=[vmem] * 6,
-            out_specs=(vmem,) * 6,
-            compiler_params=pltpu.CompilerParams(vmem_limit_bytes=48 * 1024 * 1024),
+            in_specs=[
+                pl.BlockSpec((group, rows, rank), lambda i: (i, 0, 0)), stack(w_v), stack(w_o),
+                whole(R), whole(S), whole(w_v), whole(w_o), *[whole(a) for a in small],
+            ],
+            out_specs=(
+                whole(w_v), whole(w_o), whole(w_v), whole(w_o), tall(w_v), tall(w_o),
+                *[whole(a) for a in small],
+            ),
+            compiler_params=pltpu.CompilerParams(vmem_limit_bytes=60 * 1024 * 1024),
             name="update",
-        )(F, R, W_v, W_o, w_v, w_o)
-        return (*outs, n1_v, n2_v, n1_o, n2_o)
+        )(F, W_v, W_o, R, S, w_v, w_o, *small)
 
     fsp = P(("fs", "tp"), None)
     both = P("fs", "tp")

time: 83.1 us -> 78.9 us (0.949)
  local copies, waits for them, and re-layouts: 7.36 us -> 0 us
  Pallas kernels: 74.8 us -> 78.1 us
    unnamed x24 -> x0, local copies, waits for them, and re-layouts: 7.36 us -> none
    pallas_call x1, Pallas kernels: 2.35 us -> 5.7 us  [shards(): pl.pallas_call(update_kernel, grid=(fs // group,), out_shape=(sds(w_v.sha...]
where the time goes in v2:
time: 78.9 us; the launch traced here: 78.7 us
  Pallas kernels  78.1 us (99%)
    pallas_call x1, Pallas kernels, shards(): pl.pallas_call(functools.partial(exchange_kernel, fs, tp), out_shape=(sds...  72.4 us
    pallas_call x1, Pallas kernels, shards(): pl.pallas_call(update_kernel, grid=(fs // group,), out_shape=(sds(w_v.sha...  5.7 us

profile of v2, /device:TPU:0, one launch (start us, length us, event | category | flops | bytes accessed | tf_op | source)
XLA Modules:
  0.0 78.7 jit_solution(15284798748559919603)
XLA Ops:
  0.6 72.4 %exchange.1 = (bf16[8,384,256]{2,1,0:T(8,128)(2,1)}, bf16[4,2,256,256]{3,2,1,0:T(8,128)(2,1)}, bf16[4,2,128,512]{3,2,1,0:T(8,128)(2,1)}, bf16[8,32,768]{2,1,0:T(8,128)(2,1)}, f32[32,768]{1,0:T(8,128)}) custom-call(bf16[2048,2048]{1,0:T(8,128)(2,1)} %x_v.1, bf16[2048,1024]{1,0:T(8,128)(2,1)} %c_v.1, bf16[2048,1024]{1,0:T(8,128)(2,1)} %x_o.1, ...), custom_call_target="tpu_custom_call" | custom-call | tf_op jit(solution)/shard_map/exchange/pallas_call | solution.py:427
  73.0 5.7 %update.1 = (f32[256,256]{1,0:T(8,128)}, f32[128,512]{1,0:T(8,128)}, f32[256,256]{1,0:T(8,128)}, f32[128,512]{1,0:T(8,128)}, bf16[2048,256]{1,0:T(8,128)(2,1)}, ...) custom-call(bf16[8,384,256]{2,1,0:T(8,128)(2,1)} %get-tuple-element., ...), custom_call_target="tpu_custom_call" | custom-call | tf_op jit(solution)/shard_map/update/pallas_call | solution.py:453
